TPU v7x, 32 devices: a whole 2x2x4 slice. The times are simulated.
32 devices in a mesh: ep: 8 (over z, core), tp: 4 (over y, x).
Axes of the slice: x: 2, y: 2, z: 4, core: 2. Of those that a mesh axis runs over, the one named last changes fastest.
Arguments:
- tokens: bfloat16 [1024, 2048], P('ep'), may hold values from -6 to 6
- cotangent: bfloat16 [1024, 2048], P('ep'), may hold values from -6 to 6
- expert_ids: int32 [1024, 2], P('ep'), may hold values from 0 to 7, all different within a row; in each aligned block of 128 rows (0 to 127, 128 to 255, ...) at most 64 rows name the same one
- route_weight: bfloat16 [1024, 2], P('ep'), may hold values from 0.19921875 to 1
- gate_weight: bfloat16 [8, 1024, 2048], P('ep', 'tp'), may hold values from -0.125 to 0.125
- up_weight: bfloat16 [8, 1024, 2048], P('ep', 'tp'), may hold values from -0.125 to 0.125
- down_weight: bfloat16 [8, 1024, 2048], P('ep', 'tp'), may hold values from -0.1875 to 0.1875
Outputs:
- tokens_grad: bfloat16 [1024, 2048], P('ep', 'tp')
- route_weight_grad: float32 [1024, 2], P('ep')
- gate_weight_grad: float32 [8, 1024, 2048], P('ep', 'tp')
- up_weight_grad: float32 [8, 1024, 2048], P('ep', 'tp')
- down_weight_grad: float32 [8, 1024, 2048], P('ep', 'tp')
Inputs may be any that keep to these rules, and one draw needn't show every extreme that they name: `expert_ids`: within each aligned block of 128 rows every expert is named at most 64 times; the two experts of a row differ.
All inputs are finite; a program needn't handle non-finite values.
Results may differ from a plain program's by a relative error of at most 0.0058.
Values may be sent and summed in bfloat16 or wider, within the bound.
A program may use at most 64 MiB of HBM per device.

v0:
```python
import jax
import jax.numpy as jnp
from jax import lax
from jax.sharding import PartitionSpec as P


def per_device(tokens, cotangent, expert_ids, route_weight, gate_weight, up_weight, down_weight):
    tok_rows, model_width = tokens.shape
    top_count = expert_ids.shape[1]
    local_experts = gate_weight.shape[0]
    ep_size = lax.axis_size("ep")
    tp_size = lax.axis_size("tp")
    expert_count = local_experts * ep_size
    capacity = 2 * tok_rows * top_count // expert_count
    column_span = model_width // tp_size
    flat_ids = expert_ids.reshape(-1)
    routed = flat_ids.shape[0]
    member = (flat_ids[:, None] == jnp.arange(expert_count, dtype=jnp.int32)[None, :]).astype(
        jnp.int32
    )
    rank_slot = jnp.sum((jnp.cumsum(member, axis=0) - 1) * member, axis=1)
    slot_index = flat_ids * capacity + rank_slot
    buffer_rows = expert_count * capacity
    source_pair = (
        jnp.full((buffer_rows,), routed, jnp.int32)
        .at[slot_index]
        .set(jnp.arange(routed, dtype=jnp.int32))
    )
    filled = source_pair < routed
    safe_pair = jnp.minimum(source_pair, routed - 1)
    token_of = safe_pair // top_count
    zero_value = jnp.zeros((), tokens.dtype)
    send_weight = jnp.where(filled, route_weight.reshape(-1)[safe_pair], zero_value)
    offset = lax.axis_index("tp") * column_span
    token_cols = lax.dynamic_slice_in_dim(tokens, offset, column_span, 1)
    cotangent_cols = lax.dynamic_slice_in_dim(cotangent, offset, column_span, 1)
    part_tokens, part_cotangent, got_weight = (
        lax.all_to_all(token_cols[token_of], "ep", split_axis=0, concat_axis=0, tiled=True),
        lax.all_to_all(cotangent_cols[token_of], "ep", split_axis=0, concat_axis=0, tiled=True),
        lax.all_to_all(send_weight, "ep", split_axis=0, concat_axis=0, tiled=True),
    )
    got_tokens, got_cotangent = (
        lax.all_gather(part_tokens, "tp", axis=1, tiled=True),
        lax.all_gather(part_cotangent, "tp", axis=1, tiled=True),
    )
    block_shape = (ep_size, local_experts, capacity, model_width)
    routed_rows = got_tokens.reshape(block_shape)
    routed_cotangent = got_cotangent.reshape(block_shape)
    pair_weight = got_weight.reshape(ep_size, local_experts, capacity, 1).astype(jnp.float32)
    pre_gate = jnp.einsum(
        "secd,efd->secf", routed_rows, gate_weight, preferred_element_type=jnp.float32
    )
    pre_up = jnp.einsum(
        "secd,efd->secf", routed_rows, up_weight, preferred_element_type=jnp.float32
    )
    sigma = jax.nn.sigmoid(pre_gate)
    silu_gate = pre_gate * sigma
    hidden = silu_gate * pre_up
    back_hidden = jnp.einsum(
        "secd,efd->secf", routed_cotangent, down_weight, preferred_element_type=jnp.float32
    )
    pair_products = lax.psum(jnp.sum(hidden * back_hidden, axis=3), "tp")
    scaled = pair_weight * back_hidden
    grad_gate = (scaled * pre_up * sigma * (1.0 + pre_gate * (1.0 - sigma))).astype(jnp.bfloat16)
    grad_up = (scaled * silu_gate).astype(jnp.bfloat16)
    weighted = (pair_weight * hidden).astype(jnp.bfloat16)
    down_grad = jnp.einsum(
        "secf,secd->efd", weighted, routed_cotangent, preferred_element_type=jnp.float32
    )
    gate_grad = jnp.einsum(
        "secf,secd->efd", grad_gate, routed_rows, preferred_element_type=jnp.float32
    )
    up_grad = jnp.einsum("secf,secd->efd", grad_up, routed_rows, preferred_element_type=jnp.float32)
    full_gate, full_up = (
        lax.all_gather(grad_gate, "tp", axis=3, tiled=True),
        lax.all_gather(grad_up, "tp", axis=3, tiled=True),
    )
    gate_cols, up_cols = (
        lax.all_to_all(gate_weight, "tp", split_axis=2, concat_axis=1, tiled=True),
        lax.all_to_all(up_weight, "tp", split_axis=2, concat_axis=1, tiled=True),
    )
    pair_grad = (
        jnp.einsum("secf,efd->secd", full_gate, gate_cols, preferred_element_type=jnp.float32)
        + jnp.einsum("secf,efd->secd", full_up, up_cols, preferred_element_type=jnp.float32)
    ).astype(jnp.bfloat16)
    returned = lax.all_to_all(
        pair_grad.reshape(buffer_rows, column_span), "ep", split_axis=0, concat_axis=0, tiled=True
    )
    returned_products = lax.all_to_all(
        pair_products.reshape(buffer_rows), "ep", split_axis=0, concat_axis=0, tiled=True
    )
    per_pair = returned[slot_index].astype(jnp.float32).reshape(tok_rows, top_count, column_span)
    tokens_grad = jnp.sum(per_pair, axis=1).astype(jnp.bfloat16)
    route_grad = returned_products[slot_index].reshape(tok_rows, top_count)
    return (tokens_grad, route_grad, gate_grad, up_grad, down_grad)


def solution(mesh):
    in_specs = (
        P("ep", None),
        P("ep", None),
        P("ep", None),
        P("ep", None),
        P("ep", "tp", None),
        P("ep", "tp", None),
        P("ep", "tp", None),
    )
    out_specs = (
        P("ep", "tp"),
        P("ep", None),
        P("ep", "tp", None),
        P("ep", "tp", None),
        P("ep", "tp", None),
    )
    return jax.shard_map(
        per_device, mesh=mesh, in_specs=in_specs, out_specs=out_specs, check_vma=False
    )
```

profile of v0, /device:TPU:0, one launch (start us, length us, event | category | flops | bytes accessed | tf_op | source)
XLA Modules:
  0.0 231.4 jit_solution(7355271830630326382)
XLA Ops:
  14.7 21.6 %all_to_all.85 = bf16[8,64,512]{2,1,0:T(8,128)(2,1)} all-to-all(bf16[8,64,512]{2,1,0:T(8,128)(2,1)S(1)} %bitcast.112), channel_id=1, replica_groups=mesh['ep'=8,'tp'=4] {'ep'}, dimensions={0} | all-to-all | bytes 1048576 | tf_op jit(solution)/shard_map/all_to_all | solution.py:38
  38.4 18.5 %all_to_all.86 = bf16[8,64,512]{2,1,0:T(8,128)(2,1)} all-to-all(bf16[8,64,512]{2,1,0:T(8,128)(2,1)S(1)} %bitcast.111), channel_id=1, replica_groups=mesh['ep'=8,'tp'=4] {'ep'}, dimensions={0} | all-to-all | bytes 1048576 | tf_op jit(solution)/shard_map/all_to_all | solution.py:39
  57.3 3.4 %gather_fusion = bf16[512]{0:T(512)(128)(2,1)S(1)} fusion(bf16[256]{0:T(256)(128)(2,1)S(1)} %reshape.155, s32[1024]{0:T(1024)S(1)} %get-tuple-element.28), kind=kCustom, calls=%fused_computation | custom fusion | bytes 4096 | tf_op jit(solution)/shard_map/gather | solution.py:33
  60.8 8.1 %all_to_all.87 = bf16[8,64,1]{1,2,0:T(2,128)(2,1)S(1)} all-to-all(bf16[8,64,1]{1,2,0:T(2,128)(2,1)S(1)} %all_to_all.77), channel_id=1, replica_groups=mesh['ep'=8,'tp'=4] {'ep'}, dimensions={0} | all-to-all | bytes 2048 | tf_op jit(solution)/shard_map/all_to_all | solution.py:40
  70.5 3.3 %convolution_bitcast_fusion.4 = f32[8,1,64,256]{3,2,0,1:T(8,128)} fusion(bf16[8,64,2048]{2,1,0:T(8,128)(2,1)} %bitcast.101, bf16[1,256,2048]{2,1,0:T(8,128)(2,1)S(1)} %copy-done.5), kind=kOutput, calls=%fused_computation.12 | convolution fusion | flops 536870912 | bytes 3670016 | tf_op jit(solution)/shard_map/secd,efd->secf/dot_general | solution.py:53
  74.5 32.8 %all-gather.5.cloned.1.call-done = bf16[512,2048]{1,0:T(8,128)(2,1)} async-done(((bf16[512,512]{1,0:T(8,128)(2,1)}), bf16[512,2048]{1,0:T(8,128)(2,1)}) %all-gather.5.cloned.1.call-update) | async-done | bytes 2097168 | tf_op jit(solution)/shard_map/all_gather | solution.py:44
  107.4 3.3 %multiply_reduce_fusion = (f32[8,64]{1,0:T(8,128)S(1)}, bf16[8,1,64,256]{3,2,0,1:T(8,128)(2,1)}, bf16[8,1,64,256]{3,2,0,1:T(8,128)(2,1)}) fusion(f32[8,1,64,256]{3,2,0,1:T(8,128)S(1)} %copy-done.9, f32[8,1,64,256]{3,2,0,1:T(8,128)S(1)} %convolution_bitcast_fusion.3, f32[8,64]{1,0:T(8,128)S(1)} %bitcast.117, bf16[8,64,2048]{2,1,0:T(8,128)(2,1)} %bitcast.109, ...), kind=kOutput, calls=%fused_computation.21 | convolution fusion | flops 539098624 | bytes 4722688 | tf_op jit(solution)/shard_map/secd,efd->secf/dot_general | solution.py:59
  110.6 4.6 %copy.35 = bf16[1,256,2048]{1,0,2:T(2,128)(2,1)S(1)} copy(bf16[1,256,2048]{2,1,0:T(8,128)(2,1)} %param.11) | data formatting | bytes 2097152 | tf_op args[4]
  115.8 11.6 %reduce.8 = bf16[2048,256]{1,0:T(8,128)(2,1)} reduce(bf16[2048,1,256]{2,1,0:T(2,128)(2,1)S(1)} %bitcast.105, bf16[]{:T(256)} %broadcast.123), dimensions={1}, to_apply=%bitcast.84.reduce_sub_computation | reduce | bytes 2097154
  127.3 3.5 %reshape.242 = bf16[4,2,65536]{2,1,0:T(2,128)(2,1)} reshape(bf16[2048,256]{1,0:T(8,128)(2,1)} %reduce.8) | data formatting | bytes 2097152
  130.8 4.2 %all-to-all-start.3 = ((bf16[4,2,65536]{2,1,0:T(2,128)(2,1)}), bf16[4,2,65536]{2,1,0:T(2,128)(2,1)}, u32[]{:S(2)}, u32[]{:S(2)}) async-start(bf16[4,2,65536]{2,1,0:T(2,128)(2,1)} %reshape.242), calls=%async_computation.3 | async-start | bytes 2097152 | tf_op jit(solution)/shard_map/all_to_all | solution.py:79
  135.6 4.6 %copy.37 = bf16[1,256,2048]{1,0,2:T(2,128)(2,1)S(1)} copy(bf16[1,256,2048]{2,1,0:T(8,128)(2,1)} %param.12) | data formatting | bytes 2097152 | tf_op args[5]
  140.3 11.6 %reduce.9 = bf16[2048,256]{1,0:T(8,128)(2,1)} reduce(bf16[2048,1,256]{2,1,0:T(2,128)(2,1)S(1)} %bitcast.106, bf16[]{:T(256)} %broadcast.123), dimensions={1}, to_apply=%bitcast.86.reduce_sub_computation | reduce | bytes 2097154
  151.8 3.5 %reshape.244 = bf16[4,2,65536]{2,1,0:T(2,128)(2,1)} reshape(bf16[2048,256]{1,0:T(8,128)(2,1)} %reduce.9) | data formatting | bytes 2097152
  155.3 4.3 %all-to-all-start.4 = ((bf16[4,2,65536]{2,1,0:T(2,128)(2,1)}), bf16[4,2,65536]{2,1,0:T(2,128)(2,1)}, u32[]{:S(2)}, u32[]{:S(2)}) async-start(bf16[4,2,65536]{2,1,0:T(2,128)(2,1)} %reshape.244), calls=%async_computation.4 | async-start | bytes 2097152 | tf_op jit(solution)/shard_map/all_to_all | solution.py:80
  159.6 2.6 %reshape.243 = bf16[2048,1,256]{2,1,0:T(2,128)(2,1)S(1)} reshape(bf16[4,2,65536]{2,1,0:T(2,128)(2,1)} %all-to-all-done.3) | data formatting | bytes 2097152
  165.6 10.7 %all-to-all-done.4 = bf16[4,2,65536]{2,1,0:T(2,128)(2,1)} async-done(((bf16[4,2,65536]{2,1,0:T(2,128)(2,1)}), bf16[4,2,65536]{2,1,0:T(2,128)(2,1)}, u32[]{:S(2)}, u32[]{:S(2)}) %all-to-all-start.4) | async-done | bytes 1048608 | tf_op jit(solution)/shard_map/all_to_all | solution.py:80
  181.7 9.5 %psum.7 = f32[8,64,1]{1,2,0:T(1,128)} all-reduce(f32[8,64,1]{1,2,0:T(1,128)S(1)} %bitcast.121), channel_id=1, replica_groups=mesh['ep'=8,'tp'=4] {'tp'}, use_global_device_ids=true, to_apply=%region_6.7 | all-reduce | flops 512 | bytes 4096 | tf_op jit(solution)/shard_map/psum | solution.py:62
  191.3 4.6 %all-to-all-start.6 = ((f32[8,64,1]{1,2,0:T(1,128)}), f32[8,64,1]{1,2,0:T(1,128)S(1)}, u32[]{:S(2)}, u32[]{:S(2)}) async-start(f32[8,64,1]{1,2,0:T(1,128)} %psum.7), calls=%async_computation.6 | async-start | bytes 8192 | tf_op jit(solution)/shard_map/all_to_all | solution.py:89
  195.9 2.9 %fusion.2 = f32[8,64,512]{2,1,0:T(8,128)} fusion(bf16[1024,512,1]{1,0,2:T(8,128)(2,1)S(1)} %bitcast.115, bf16[8,1,64,1024]{3,2,0,1:T(8,128)(2,1)} %all-gather.9.cloned.1.call-done), kind=kOutput, calls=%fused_computation.15 | convolution fusion | flops 536870912 | bytes 3145728 | tf_op jit(solution)/shard_map/secf,efd->secd/dot_general | solution.py:83
  198.8 3.1 %fusion = bf16[8,64,512]{2,1,0:T(8,128)(2,1)} fusion(f32[8,64,512]{2,1,0:T(8,128)} %fusion.2, bf16[1024,512,1]{1,0,2:T(8,128)(2,1)S(1)} %bitcast.116, bf16[8,1,64,1024]{3,2,0,1:T(8,128)(2,1)} %all-gather.11.cloned.1.call-done), kind=kOutput, calls=%fused_computation.10 | convolution fusion | flops 537395200 | bytes 3670016 | tf_op jit(solution)/shard_map/secf,efd->secd/dot_general | solution.py:84
  201.9 5.1 %all-to-all-start.5 = ((bf16[8,64,512]{2,1,0:T(8,128)(2,1)}), bf16[8,64,512]{2,1,0:T(8,128)(2,1)S(1)}, u32[]{:S(2)}, u32[]{:S(2)}) async-start(bf16[8,64,512]{2,1,0:T(8,128)(2,1)} %fusion), calls=%async_computation.5 | async-start | bytes 1048576 | tf_op jit(solution)/shard_map/all_to_all | solution.py:86
  207.0 3.8 %convolution_bitcast_fusion.2 = f32[1,256,2048]{2,1,0:T(8,128)} fusion(bf16[8,64,2048]{2,1,0:T(8,128)(2,1)} %bitcast.102, bf16[8,1,64,256]{3,2,0,1:T(8,128)(2,1)S(1)} %copy-done.7), kind=kOutput, calls=%fused_computation.8 | convolution fusion | flops 536870912 | bytes 4456448 | tf_op jit(solution)/shard_map/secf,secd->efd/dot_general | solution.py:70
  219.2 3.1 %all-to-all-done.5 = bf16[8,64,512]{2,1,0:T(8,128)(2,1)S(1)} async-done(((bf16[8,64,512]{2,1,0:T(8,128)(2,1)}), bf16[8,64,512]{2,1,0:T(8,128)(2,1)S(1)}, u32[]{:S(2)}, u32[]{:S(2)}) %all-to-all-start.5) | async-done | bytes 524320 | tf_op jit(solution)/shard_map/all_to_all | solution.py:86
  (85 shorter events, 33.2 us)
Async XLA Ops:
  7.2 100.2 %copy-start = (bf16[1,256,2048]{2,1,0:T(8,128)(2,1)S(1)}, bf16[1,256,2048]{2,1,0:T(8,128)(2,1)}, u32[]{:S(2)}) copy-start(bf16[1,256,2048]{2,1,0:T(8,128)(2,1)} %param.13) | copy-start | bytes 3145732
  7.2 63.3 %all-gather.7.cloned.1.call-start = ((), (), s32[]{:S(2)}) async-start(), calls=%async_computation.8 | async-start | bytes 2621440 | tf_op jit(solution)/shard_map/all_gather | solution.py:43
  36.3 71.0 %all-gather.5.cloned.1.call-start = ((), (), s32[]{:S(2)}) async-start(), calls=%async_computation.7 | async-start | bytes 2621440 | tf_op jit(solution)/shard_map/all_gather | solution.py:44
  36.4 20.6 %copy-start.13 = (bf16[128,2]{0,1:T(2,128)(2,1)S(1)}, bf16[128,2]{0,1:T(2,128)(2,1)}, u32[]{:S(2)}) copy-start(bf16[128,2]{0,1:T(2,128)(2,1)} %param.10) | copy-start | bytes 1540
  38.4 32.1 %copy-start.5 = (bf16[1,256,2048]{2,1,0:T(8,128)(2,1)S(1)}, bf16[1,256,2048]{2,1,0:T(8,128)(2,1)}, u32[]{:S(2)}) copy-start(bf16[1,256,2048]{2,1,0:T(8,128)(2,1)} %param.12) | copy-start | bytes 3145732
  56.9 138.9 %all-gather.9.cloned.1.call-start = ((), (), s32[]{:S(2)}) async-start(), calls=%async_computation.9 | async-start | bytes 1310720 | tf_op jit(solution)/shard_map/all_gather | solution.py:75
  60.7 13.1 %copy-start.4 = (bf16[1,256,2048]{2,1,0:T(8,128)(2,1)S(1)}, bf16[1,256,2048]{2,1,0:T(8,128)(2,1)}, u32[]{:S(2)}) copy-start(bf16[1,256,2048]{2,1,0:T(8,128)(2,1)} %param.11) | copy-start | bytes 3145732
  70.5 3.3 %copy-start.1 = (bf16[512,2048]{1,0:T(8,128)(2,1)S(1)}, bf16[512,2048]{1,0:T(8,128)(2,1)}, u32[]{:S(2)}) copy-start(bf16[512,2048]{1,0:T(8,128)(2,1)} %all-gather.7.cloned.1.call-done) | copy-start | bytes 6291460
  73.8 33.6 %copy-start.9 = (f32[8,1,64,256]{3,2,0,1:T(8,128)S(1)}, f32[8,1,64,256]{3,2,0,1:T(8,128)}, u32[]{:S(2)}) copy-start(f32[8,1,64,256]{3,2,0,1:T(8,128)} %convolution_bitcast_fusion.4) | copy-start | bytes 1572868
  74.5 36.1 %copy-start.11 = (f32[8,1,64,256]{3,2,0,1:T(8,128)}, f32[8,1,64,256]{3,2,0,1:T(8,128)S(1)}, u32[]{:S(2)}) copy-start(f32[8,1,64,256]{3,2,0,1:T(8,128)S(1)} %convolution_bitcast_fusion.3) | copy-start | bytes 1572868
  130.8 24.5 %all-to-all-start.3 = ((bf16[4,2,65536]{2,1,0:T(2,128)(2,1)}), bf16[4,2,65536]{2,1,0:T(2,128)(2,1)}, u32[]{:S(2)}, u32[]{:S(2)}) async-start(bf16[4,2,65536]{2,1,0:T(2,128)(2,1)} %reshape.242), calls=%async_computation.3 | async-start | bytes 2097152 | tf_op jit(solution)/shard_map/all_to_all | solution.py:79
  135.1 63.7 %all-gather.11.cloned.1.call-start = ((), (), s32[]{:S(2)}) async-start(), calls=%async_computation.10 | async-start | bytes 1310720 | tf_op jit(solution)/shard_map/all_gather | solution.py:76
  155.3 21.1 %all-to-all-start.4 = ((bf16[4,2,65536]{2,1,0:T(2,128)(2,1)}), bf16[4,2,65536]{2,1,0:T(2,128)(2,1)}, u32[]{:S(2)}, u32[]{:S(2)}) async-start(bf16[4,2,65536]{2,1,0:T(2,128)(2,1)} %reshape.244), calls=%async_computation.4 | async-start | bytes 2097152 | tf_op jit(solution)/shard_map/all_to_all | solution.py:80
  180.1 15.7 %copy-start.8 = (bf16[1,4,256,512]{3,2,1,0:T(8,128)(2,1)S(1)}, bf16[1,4,256,512]{3,2,1,0:T(8,128)(2,1)}, u32[]{:S(2)}) copy-start(bf16[1,4,256,512]{3,2,1,0:T(8,128)(2,1)} %copy.36) | copy-start | bytes 3145732
  191.3 10.6 %all-to-all-start.6 = ((f32[8,64,1]{1,2,0:T(1,128)}), f32[8,64,1]{1,2,0:T(1,128)S(1)}, u32[]{:S(2)}, u32[]{:S(2)}) async-start(f32[8,64,1]{1,2,0:T(1,128)} %psum.7), calls=%async_computation.6 | async-start | bytes 8192 | tf_op jit(solution)/shard_map/all_to_all | solution.py:89
  198.8 8.2 %copy-start.7 = (bf16[8,1,64,256]{3,2,0,1:T(8,128)(2,1)S(1)}, bf16[8,1,64,256]{3,2,0,1:T(8,128)(2,1)}, u32[]{:S(2)}) copy-start(bf16[8,1,64,256]{3,2,0,1:T(8,128)(2,1)} %get-tuple-element.21) | copy-start | bytes 786436
  201.9 20.4 %all-to-all-start.5 = ((bf16[8,64,512]{2,1,0:T(8,128)(2,1)}), bf16[8,64,512]{2,1,0:T(8,128)(2,1)S(1)}, u32[]{:S(2)}, u32[]{:S(2)}) async-start(bf16[8,64,512]{2,1,0:T(8,128)(2,1)} %fusion), calls=%async_computation.5 | async-start | bytes 1048576 | tf_op jit(solution)/shard_map/all_to_all | solution.py:86
  207.0 3.8 %copy-start.2 = (bf16[512,2048]{1,0:T(8,128)(2,1)S(1)}, bf16[512,2048]{1,0:T(8,128)(2,1)}, u32[]{:S(2)}) copy-start(bf16[512,2048]{1,0:T(8,128)(2,1)} %all-gather.7.cloned.1.call-done) | copy-start | bytes 6291460
  207.0 3.8 %copy-start.6 = (bf16[8,1,64,256]{3,2,0,1:T(8,128)(2,1)S(1)}, bf16[8,1,64,256]{3,2,0,1:T(8,128)(2,1)}, u32[]{:S(2)}) copy-start(bf16[8,1,64,256]{3,2,0,1:T(8,128)(2,1)} %get-tuple-element.22) | copy-start | bytes 786436
  210.8 2.1 copy-start.3
  210.8 2.1 copy-start.10
  210.8 2.3 copy-start.12
Sparse Core Ops, SparseCore 0:
  36.4 33.9 all-gather.6
  72.3 35.0 all-gather.4
  110.8 26.3 all-gather.8
  138.8 34.8 all-gather.10
where the time goes:
time: 233 us; the launch traced here: 231 us
  blocking collectives  57.7 us (25%)
  waiting for transfers between devices  48.6 us (21%)
  local copies, waits for them, and re-layouts  44.5 us (19%)
  other arithmetic  26.7 us (11%)
  matrix products  21.3 us (9%)
  starting transfers between devices  18.5 us (8%)
  between operations  14.1 us (6%)
    all_gather x1, waiting for transfers between devices, per_device(): lax.all_gather(part_cotangent, 'tp', axis=1, tiled=True)  32.8 us
    unnamed x40, local copies, waits for them, and re-layouts  26 us
    unnamed x2, other arithmetic  23.1 us
    all_to_all x1, blocking collectives, per_device(): lax.all_to_all(token_cols[token_of], 'ep', split_axis=0, concat_axis=0, t...  21.6 us
    all_to_all x1, blocking collectives, per_device(): lax.all_to_all(cotangent_cols[token_of], 'ep', split_axis=0, concat_axis=...  18.5 us
    all_to_all x1, waiting for transfers between devices, per_device(): lax.all_to_all(up_weight, 'tp', split_axis=2, concat_axis=1, tiled=True)  10.7 us
    psum x1, blocking collectives, per_device(): pair_products = lax.psum(jnp.sum(hidden * back_hidden, axis=3), 'tp')  9.53 us
    all_to_all x1, blocking collectives, per_device(): lax.all_to_all(send_weight, 'ep', split_axis=0, concat_axis=0, tiled=True)  8.07 us
  transfers between devices with their start and end apart: 8, of which 4 were waited for; matrix products, arithmetic and copies ran while one was open for 34% of the time, Pallas kernels for 0%

commit v1 on v0

v1 whole, which is shorter than its diff:
```python
import functools

import jax
import jax.numpy as jnp
from jax import lax
from jax.experimental import pallas as pl
from jax.experimental.pallas import tpu as pltpu
from jax.sharding import PartitionSpec as P

MESH = pl.DeviceIdType.MESH
F32 = jnp.float32
BF16 = jnp.bfloat16


def slices_for(j, tp, bits, count):
    base = j
    for bit in bits:
        base = base - ((j // bit) % 2) * bit
    out = []
    for k in range(count):
        out.append(base + sum(bit for n, bit in enumerate(bits) if (k >> n) & 1))
    return out


def kernel(
    ep, tp, tokens, cotangent, pair_w, gate_w, up_w, down_w,
    dx_out, route_out, gate_out, up_out, down_out,
    rows, weights, wg, part, core_in, tp_in, z_in, grads, totals, r_send, r_in, r_tp,
    load_sem, wz_send, wz_recv, z_send, z_recv, t_send, t_recv, c_send, c_recv,
    pc_send, pc_recv, pt_send, pt_recv, pz_send, pz_recv, rs_send, rs_recv, rt_send, rt_recv, out_sem,
):
    e, j = lax.axis_index("ep"), lax.axis_index("tp")
    levels = ep // 2
    lvl, core = e // 2, e % 2
    t_rows, width = tokens.shape
    span = width // tp
    half = t_rows // 2
    f_rows = gate_w.shape[0]
    nb = tp.bit_length() - 1
    slots = part.shape[0]
    mate = 2 * lvl + 1 - core

    def order(i):
        near = jnp.minimum(lvl, levels - 1 - lvl)
        d = (i + 1) // 2
        close = jnp.where(i % 2 == 1, lvl - d, lvl + d)
        far = jnp.where(lvl == near, lvl + (i - near), lvl - (i - near))
        return jnp.where(i <= 2 * near, close, far)

    def row0(l, c):
        return pl.multiple_of((2 * l + c) * t_rows, t_rows)

    def col(s):
        return pl.ds(pl.multiple_of(s * span, span), span)

    def flip(bit):
        return j + bit * (1 - 2 * ((j // bit) % 2))

    def remote(src, dst, ssem, rsem, de, dt):
        return pltpu.make_async_remote_copy(
            src_ref=src, dst_ref=dst, send_sem=ssem, recv_sem=rsem,
            device_id=(de, dt), device_id_type=MESH)

    own = pl.ds(row0(lvl, core), t_rows)
    loads = [
        pltpu.make_async_copy(tokens, rows.at[0, own], load_sem.at[0]),
        pltpu.make_async_copy(cotangent, rows.at[1, own], load_sem.at[1]),
        pltpu.make_async_copy(gate_w, weights.at[0], load_sem.at[2]),
        pltpu.make_async_copy(up_w, weights.at[1], load_sem.at[3]),
        pltpu.make_async_copy(down_w, weights.at[2], load_sem.at[4]),
    ]
    for copy in loads:
        copy.start()
    barrier = pltpu.get_barrier_semaphore()

    def greet(n, _):
        pl.semaphore_signal(barrier, inc=1, device_id=(lax.rem(e + n, ep), j), device_id_type=MESH)
        return 0

    def greet_tp(n, _):
        pl.semaphore_signal(barrier, inc=1, device_id=(e, lax.rem(j + n, tp)), device_id_type=MESH)
        return 0

    lax.fori_loop(1, ep, greet, 0)
    lax.fori_loop(1, tp, greet_tp, 0)
    pl.semaphore_wait(barrier, ep + tp - 2)

    def w_copy(d):
        return remote(pair_w.at[d], wg.at[e], wz_send.at[d], wz_recv.at[e], d, j)

    def w_wait(src):
        return remote(pair_w.at[src], wg.at[src], wz_send.at[src], wz_recv.at[src], src, j)

    def z_copy(a, l, side):
        ref = rows.at[a, pl.ds(row0(l, core), t_rows), col(j)]
        de = lax.rem(e + (2 if side else ep - 2), ep)
        return remote(ref, ref, z_send.at[a, side, l], z_recv.at[a, l], de, j)

    def gather_step(a, l, s, receive):
        copies = []
        for h in range(2):
            order_bits = [1 << b for b in (range(nb) if h == 0 else range(nb - 1, -1, -1))]
            peer = flip(order_bits[s])
            ids = slices_for(peer if receive else j, tp, order_bits[:s], 1 << s)
            for k, sid in enumerate(ids):
                ref = rows.at[a, pl.ds(row0(l, core) + h * half, half), col(sid)]
                copies.append(remote(
                    ref, ref, t_send.at[a, l, h, (1 << s) - 1 + k], t_recv.at[a, l, h, sid], e, peer))
        return copies

    def core_copy(a, l, c):
        ref = rows.at[a, pl.ds(row0(l, c), t_rows)]
        return remote(ref, ref, c_send.at[a, l], c_recv.at[a, l], mate, j)

    def pc_copy(l, i):
        return remote(part.at[i % slots, 1 - core], core_in.at[l], pc_send.at[l], pc_recv.at[l], mate, j)

    def scatter_step(l, i, s, receive):
        copies = []
        base = sum(tp >> (n + 1) for n in range(s))
        count = tp >> (s + 1)
        for h in range(2):
            order_bits = [1 << b for b in (range(nb) if h == 0 else range(nb - 1, -1, -1))]
            peer = flip(order_bits[s])
            ids = slices_for(j if receive else peer, tp, order_bits[s + 1:], count)
            for k, sid in enumerate(ids):
                src = part.at[i % slots, core, pl.ds(h * half, half), col(sid)]
                dst = tp_in.at[l, h, base + k]
                copies.append((remote(src, dst, pt_send.at[l, h, base + k], pt_recv.at[l, h, base + k], e, peer),
                               src, dst))
        return copies

    def pz_copy(l, i):
        return remote(part.at[i % slots, core, :, col(j)], z_in.at[lvl], pz_send.at[l], pz_recv.at[lvl],
                      2 * l + core, j)

    def pz_wait(src):
        return remote(part.at[0, core, :, col(j)], z_in.at[src], pz_send.at[src], pz_recv.at[src],
                      2 * src + core, j)

    for n in range(2):
        loads[n].wait()
        @pl.when(lvl + 1 < levels)
        def _():
            z_copy(n, lvl, 1).start()
        @pl.when(lvl > 0)
        def _():
            z_copy(n, lvl, 0).start()
        core_copy(n, lvl, core).start()

    def w_start(n, _):
        w_copy(lax.rem(e + n, ep)).start()
        return 0

    lax.fori_loop(1, ep, w_start, 0)
    wg[e] = pair_w[e]
    for n in range(2, 5):
        loads[n].wait()

    def arrive(i):
        l = order(i)
        for a in range(2):
            z_copy(a, l, 0).wait_recv()
            @pl.when(jnp.logical_and(l < lvl, lvl + 1 < levels))
            def _():
                z_copy(a, l, 1).start()
            @pl.when(jnp.logical_and(l > lvl, lvl > 0))
            def _():
                z_copy(a, l, 0).start()
            for copy in gather_step(a, l, 0, False):
                copy.start()

    def spread(i, s):
        l = order(i)
        for a in range(2):
            for copy in gather_step(a, l, s - 1, True):
                copy.wait_recv()
            if s < nb:
                for copy in gather_step(a, l, s, False):
                    copy.start()
            else:
                core_copy(a, l, core).start()

    def compute(i):
        l = order(i)
        for a in range(2):
            core_copy(a, l, 1 - core).wait_recv()
        @pl.when(l != lvl)
        def _():
            w_wait(2 * l).wait_recv()
            w_wait(2 * l + 1).wait_recv()
        @pl.when(l == lvl)
        def _():
            w_wait(mate).wait_recv()
        sel = pl.ds(row0(l, 0), 2 * t_rows)
        nt = (((1,), (1,)), ((), ()))
        x = rows[0, sel, :]
        pre_gate = lax.dot_general(weights[0], x, nt, preferred_element_type=F32)
        pre_up = lax.dot_general(weights[1], x, nt, preferred_element_type=F32)
        back = lax.dot_general(weights[2], rows[1, sel, :], nt, preferred_element_type=F32)
        p = jnp.concatenate([wg[2 * l], wg[2 * l + 1]], axis=1)
        sigma = jax.nn.sigmoid(pre_gate)
        silu = pre_gate * sigma
        hidden = silu * pre_up
        prod = jnp.sum(hidden * back, axis=0, keepdims=True)
        r_send[2 * l] = prod[:, :t_rows]
        r_send[2 * l + 1] = prod[:, t_rows:]
        scaled = p * back
        gg = (scaled * pre_up * sigma * (1.0 + pre_gate * (1.0 - sigma))).astype(BF16)
        gu = (scaled * silu).astype(BF16)
        grads[0, :, sel] = gg
        grads[1, :, sel] = gu
        grads[2, :, sel] = (p * hidden).astype(BF16)
        ggt, gut = gg.T, gu.T
        tile = min(width, 512)

        def column(n, _):
            cs = pl.ds(pl.multiple_of(n * tile, tile), tile)
            d = (jnp.dot(ggt, weights[0, :, cs], preferred_element_type=F32)
                 + jnp.dot(gut, weights[1, :, cs], preferred_element_type=F32)).astype(BF16)
            part[i % slots, 0, :, cs] = d[:t_rows]
            part[i % slots, 1, :, cs] = d[t_rows:]
            return 0

        lax.fori_loop(0, width // tile, column, 0)
        pc_copy(l, i).start()

        def send_r(d):
            remote(r_send.at[d], r_in.at[e], rs_send.at[d], rs_recv.at[e], d, j).start()
        for c in range(2):
            @pl.when(2 * l + c != e)
            def _():
                send_r(2 * l + c)
            @pl.when(2 * l + c == e)
            def _():
                r_in[2 * l + c] = r_send[2 * l + c]

    def merge_core(i):
        l = order(i)
        pc_copy(l, i).wait()
        part[i % slots, core] = (part[i % slots, core].astype(F32) + core_in[l].astype(F32)).astype(BF16)
        for copy, _, _ in scatter_step(l, i, 0, False):
            copy.start()

    def merge_tp(i, s):
        l = order(i)
        for (copy, _, _), (_, mine, got) in zip(scatter_step(l, i, s, False), scatter_step(l, i, s, True)):
            copy.wait()
            mine[...] = (mine[...].astype(F32) + got[...].astype(F32)).astype(BF16)
        if s + 1 < nb:
            for copy, _, _ in scatter_step(l, i, s + 1, False):
                copy.start()
        else:
            @pl.when(l != lvl)
            def _():
                pz_copy(l, i).start()
            @pl.when(l == lvl)
            def _():
                z_in[lvl] = part[i % slots, core, :, col(j)]

    def drain(i):
        l = order(i)
        @pl.when(l != lvl)
        def _():
            pz_copy(l, i).wait_send()

    outs = (gate_out, up_out, down_out)

    def out_copy(k):
        return pltpu.make_async_copy(totals.at[k], outs[k], out_sem.at[k])

    def weight_grad(k):
        tile = min(width, 512)

        def column(n, _):
            cs = pl.ds(pl.multiple_of(n * tile, tile), tile)
            totals[k, :, cs] = jnp.dot(grads[k], rows[k // 2, :, cs], preferred_element_type=F32)
            return 0

        lax.fori_loop(0, width // tile, column, 0)
        out_copy(k).start()

    compute(0)
    d_comp = nb + 2
    last = levels - 1 + d_comp

    def tick(t, _):
        def stage(f, i, low):
            @pl.when(jnp.logical_and(i >= low, i < levels))
            def _():
                f(i)
        def back(late):
            return jnp.where(t == 1 + late, 0, jnp.where(t > d_comp + late, t - d_comp - late, -1))

        stage(drain, back(nb + 1), 0)
        for s in range(nb - 1, -1, -1):
            stage(functools.partial(merge_tp, s=s), back(1 + s), 0)
        stage(arrive, t, 1)
        for s in range(1, nb + 1):
            stage(functools.partial(spread, s=s), t - s, 1)
        stage(compute, t - d_comp + 1, 1)
        stage(merge_core, back(0), 0)
        for k in range(3):
            @pl.when(t == last + k)
            def _():
                weight_grad(k)
        return 0

    lax.fori_loop(1, levels + d_comp + nb + 1, tick, 0)

    def r_wait(n, _):
        src = lax.rem(e + n, ep)
        remote(r_send.at[src], r_in.at[src], rs_send.at[src], rs_recv.at[src], src, j).wait()
        return 0

    lax.fori_loop(1, ep, r_wait, 0)

    def rt_copy(n):
        dt = lax.rem(j + n, tp)
        return remote(r_in, r_tp.at[j], rt_send.at[dt], rt_recv.at[j], e, dt)

    def rt_wait(n, _):
        src = lax.rem(j + n, tp)
        remote(r_in, r_tp.at[src], rt_send.at[src], rt_recv.at[src], e, src).wait()
        return 0

    def rt_start(n, _):
        rt_copy(n).start()
        return 0

    lax.fori_loop(1, tp, rt_start, 0)
    r_tp[j] = r_in[...]

    def pz_drain(src, _):
        @pl.when(src != lvl)
        def _():
            pz_wait(src).wait_recv()
        return 0

    lax.fori_loop(0, levels, pz_drain, 0)
    dx_out[...] = jnp.sum(z_in[...].astype(F32), axis=0).astype(BF16)
    lax.fori_loop(1, tp, rt_wait, 0)
    route_out[...] = jnp.sum(r_tp[...], axis=0)

    for a in range(2):
        @pl.when(lvl + 1 < levels)
        def _():
            z_copy(a, lvl, 1).wait_send()
        @pl.when(lvl > 0)
        def _():
            z_copy(a, lvl, 0).wait_send()

    def finish(l, _):
        for a in range(2):
            core_copy(a, l, core).wait_send()
            @pl.when(jnp.logical_and(l < lvl, lvl + 1 < levels))
            def _():
                z_copy(a, l, 1).wait_send()
            @pl.when(jnp.logical_and(l > lvl, lvl > 0))
            def _():
                z_copy(a, l, 0).wait_send()
            @pl.when(l != lvl)
            def _():
                for s in range(nb):
                    for copy in gather_step(a, l, s, False):
                        copy.wait_send()
        return 0

    lax.fori_loop(0, levels, finish, 0)

    def w_done(n, _):
        w_copy(lax.rem(e + n, ep)).wait_send()
        return 0

    lax.fori_loop(1, ep, w_done, 0)
    for k in range(3):
        out_copy(k).wait()


def per_device(tokens, cotangent, expert_ids, route_weight, gate_weight, up_weight, down_weight):
    ep, tp = lax.axis_size("ep"), lax.axis_size("tp")
    t_rows, width = tokens.shape
    _, f_rows, _ = gate_weight.shape
    levels = ep // 2
    span = width // tp
    slots = min(levels, 8)
    named = expert_ids.T[:, None, :] == jnp.arange(ep, dtype=jnp.int32)[None, :, None]
    pair_w = jnp.sum(jnp.where(named, route_weight.T[:, None, :].astype(F32), 0.0), axis=0)
    pair_w = pair_w.reshape(ep, 1, t_rows)
    any_, vmem = pl.BlockSpec(memory_space=pl.ANY), pl.BlockSpec(memory_space=pltpu.VMEM)
    dma = pltpu.SemaphoreType.DMA
    big = jax.ShapeDtypeStruct((f_rows, width), F32)
    scratch = [
        pltpu.VMEM((2, ep * t_rows, width), BF16),
        pltpu.VMEM((3, f_rows, width), BF16),
        pltpu.VMEM((ep, 1, t_rows), F32),
        pltpu.VMEM((slots, 2, t_rows, width), BF16),
        pltpu.VMEM((levels, t_rows, width), BF16),
        pltpu.VMEM((levels, 2, tp - 1, t_rows // 2, span), BF16),
        pltpu.VMEM((levels, t_rows, span), BF16),
        pltpu.VMEM((3, f_rows, ep * t_rows), BF16),
        pltpu.VMEM((3, f_rows, width), F32),
        pltpu.VMEM((ep, 1, t_rows), F32),
        pltpu.VMEM((ep, 1, t_rows), F32),
        pltpu.VMEM((tp, ep, 1, t_rows), F32),
        dma((5,)), dma((ep,)), dma((ep,)), dma((2, 2, levels)), dma((2, levels)),
        dma((2, levels, 2, tp - 1)), dma((2, levels, 2, tp)), dma((2, levels)), dma((2, levels)),
        dma((levels,)), dma((levels,)), dma((levels, 2, tp - 1)), dma((levels, 2, tp - 1)),
        dma((levels,)), dma((levels,)), dma((ep,)), dma((ep,)), dma((tp,)), dma((tp,)), dma((3,)),
    ]
    dx, route, gate_grad, up_grad, down_grad = pl.pallas_call(
        functools.partial(kernel, ep, tp),
        out_shape=(
            jax.ShapeDtypeStruct((t_rows, span), BF16),
            jax.ShapeDtypeStruct((ep, 1, t_rows), F32), big, big, big),
        in_specs=[any_, any_, vmem, any_, any_, any_],
        out_specs=(vmem, vmem, any_, any_, any_),
        scratch_shapes=scratch,
        compiler_params=pltpu.CompilerParams(
            collective_id=0, has_side_effects=True, vmem_limit_bytes=66_000_000),
    )(tokens, cotangent, pair_w, gate_weight[0], up_weight[0], down_weight[0])
    route_grad = jnp.sum(jnp.where(named, route[None, :, 0, :], 0.0), axis=1).T
    return dx, route_grad, gate_grad[None], up_grad[None], down_grad[None]


def solution(mesh):
    in_specs = (
        P("ep", None), P("ep", None), P("ep", None), P("ep", None),
        P("ep", "tp", None), P("ep", "tp", None), P("ep", "tp", None),
    )
    out_specs = (
        P("ep", "tp"), P("ep", None), P("ep", "tp", None), P("ep", "tp", None), P("ep", "tp", None),
    )
    return jax.shard_map(
        per_device, mesh=mesh, in_specs=in_specs, out_specs=out_specs, check_vma=False
    )
```

time: 233 us -> 93.2 us (0.40)
  Pallas kernels: 0 us -> 80.5 us
  blocking collectives: 57.7 us -> 0 us
  waiting for transfers between devices: 48.6 us -> 0 us
  local copies, waits for them, and re-layouts: 44.5 us -> 8.52 us
  other arithmetic: 26.7 us -> 3.19 us
  matrix products: 21.3 us -> 0 us
  starting transfers between devices: 18.5 us -> 0 us
  between operations: 14.1 us -> 0.65 us
    pallas_call x0 -> x1, Pallas kernels: none -> 80.5 us  [per_device(): pl.pallas_call(functools.partial(kernel, ep, tp), out_shape=(jax.ShapeDty...]
    all_to_all x3 -> x0, blocking collectives: 48.2 us -> none  [the longest x1 21.6 us: per_device(): lax.all_to_all(token_cols[token_of], 'ep', split_axis=0, concat_axis=0, t...]
    all_gather x4 -> x0, waiting for transfers between devices: 34.4 us -> none  [the longest x1 32.8 us: per_device(): lax.all_gather(part_cotangent, 'tp', axis=1, tiled=True)]
    unnamed x2 -> x0, other arithmetic: 23.1 us -> none
    dot_general x8 -> x0, matrix products: 21.3 us -> none  [the longest x1 3.79 us: per_device(): jnp.einsum('secf,secd->efd', grad_gate, routed_rows, preferred_element_ty...]
    all_to_all x4 -> x0, starting transfers between devices: 18.2 us -> none  [the longest x1 5.07 us: per_device(): lax.all_to_all(pair_grad.reshape(buffer_rows, column_span), 'ep', split_a...]
    unnamed x40 -> x10, local copies, waits for them, and re-layouts: 26 us -> 8.52 us
    all_to_all x4 -> x0, waiting for transfers between devices: 13.8 us -> none  [the longest x1 10.7 us: per_device(): lax.all_to_all(up_weight, 'tp', split_axis=2, concat_axis=1, tiled=True)]
  transfers between devices with their start and end apart: 8 -> 0, of which waited for: 4 -> 0; matrix products, arithmetic and copies ran while one was open for 34% -> 0% of each run, Pallas kernels for 0% -> 0%
where the time goes in v1:
time: 93.2 us; the launch traced here: 92.9 us
  Pallas kernels  80.5 us (86%)
  local copies, waits for them, and re-layouts  8.52 us (9%)
  other arithmetic  3.19 us (3%)
    pallas_call x1, Pallas kernels, per_device(): pl.pallas_call(functools.partial(kernel, ep, tp), out_shape=(jax.ShapeDty...  80.5 us
    unnamed x10, local copies, waits for them, and re-layouts  8.52 us

profile of v1, /device:TPU:0, one launch (start us, length us, event | category | flops | bytes accessed | tf_op | source)
XLA Modules:
  0.0 92.9 jit_solution(17828113445888700239)
XLA Ops:
  0.6 0.7 convert_bitcast_fusion
  1.3 1.3 %select_reduce_fusion.1 = f32[8,128]{1,0:T(8,128)} fusion(f32[2,128]{1,0:T(2,128)S(1)} %convert_bitcast_fusion, s32[2,128]{1,0:T(2,128)} %bitcast.20), kind=kLoop, calls=%fused_computation.1 | loop fusion | flops 5120 | bytes 6144 | tf_op jit(solution)/shard_map/reduce_sum | solution.py:388
  2.6 0.0 copy-start.2
  2.6 80.5 %shard_map.110 = (bf16[128,512]{1,0:T(8,128)(2,1)}, f32[8,1,128]{2,1,0:T(1,128)}, f32[256,2048]{1,0:T(8,128)}, f32[256,2048]{1,0:T(8,128)}, f32[256,2048]{1,0:T(8,128)}) custom-call(bf16[128,2048]{1,0:T(8,128)(2,1)} %tokens.1, bf16[128,2048]{1,0:T(8,128)(2,1)} %cotangent.1, f32[8,1,128]{2,1,0:T(1,128)} %bitcast.18, bf16[256,2048]{1,0:T(8,128)(2,1)} %bitcast.15, ...), custom_call_target="tpu_custom_call" | custom-call | tf_op jit(solution)/shard_map/pallas_call | solution.py:411
  83.1 0.0 copy-done.2
  83.1 1.3 %select_reduce_fusion = f32[2,128]{1,0:T(2,128)} fusion(f32[8,128]{1,0:T(8,128)} %bitcast.19, s32[2,128]{1,0:T(2,128)S(1)} %bitcast.21), kind=kLoop, calls=%fused_computation | loop fusion | flops 5888 | bytes 6144 | tf_op jit(solution)/shard_map/reduce_sum | solution.py:422
  84.4 1.6 %copy.16 = bf16[128,512]{1,0:T(8,128)(2,1)} copy(bf16[128,512]{1,0:T(8,128)(2,1)} %get-tuple-element.20) | data formatting | bytes 262144
  85.9 0.0 copy-start.1
  85.9 3.3 %copy.17 = f32[1,256,2048]{2,1,0:T(8,128)} copy(f32[1,256,2048]{2,1,0:T(8,128)} %bitcast.14) | data formatting | bytes 4194304
  89.2 0.0 copy-done.1
  89.2 0.0 copy-start
  89.2 1.3 %copy.18 = f32[1,256,2048]{2,1,0:T(8,128)} copy(f32[1,256,2048]{2,1,0:T(8,128)S(1)} %bitcast.13) | data formatting | bytes 4194304
  90.6 1.0 %copy-done = f32[256,2048]{1,0:T(8,128)S(1)} copy-done((f32[256,2048]{1,0:T(8,128)S(1)}, f32[256,2048]{1,0:T(8,128)}, u32[]{:S(2)}) %copy-start) | copy-done | bytes 2097176
  91.6 1.3 %copy.19 = f32[1,256,2048]{2,1,0:T(8,128)} copy(f32[1,256,2048]{2,1,0:T(8,128)S(1)} %bitcast.12) | data formatting | bytes 4194304
Async XLA Ops:
  2.6 80.5 %copy-start.2 = (s32[128,2]{0,1:T(2,128)S(1)}, s32[128,2]{0,1:T(2,128)}, u32[]{:S(2)}) copy-start(s32[128,2]{0,1:T(2,128)} %param.9) | copy-start | bytes 3076
  85.9 3.3 %copy-start.1 = (f32[256,2048]{1,0:T(8,128)S(1)}, f32[256,2048]{1,0:T(8,128)}, u32[]{:S(2)}) copy-start(f32[256,2048]{1,0:T(8,128)} %get-tuple-element.13) | copy-start | bytes 6291460
  89.2 2.3 %copy-start = (f32[256,2048]{1,0:T(8,128)S(1)}, f32[256,2048]{1,0:T(8,128)}, u32[]{:S(2)}) copy-start(f32[256,2048]{1,0:T(8,128)} %get-tuple-element.14) | copy-start | bytes 6291460

commit v2 on v1

--- a/solution.py
+++ b/solution.py
@@ -23,9 +23,9 @@
 
 
 def kernel(
-    ep, tp, tokens, cotangent, pair_w, gate_w, up_w, down_w,
+    ep, tp, tokens, cotangent, ids, probs, gate_w, up_w, down_w,
     dx_out, route_out, gate_out, up_out, down_out,
-    rows, weights, wg, part, core_in, tp_in, z_in, grads, totals, r_send, r_in, r_tp,
+    rows, weights, pair_w, wg, part, core_in, tp_in, z_in, grads, totals, r_send, r_in, r_tp,
     load_sem, wz_send, wz_recv, z_send, z_recv, t_send, t_recv, c_send, c_recv,
     pc_send, pc_recv, pt_send, pt_recv, pz_send, pz_recv, rs_send, rs_recv, rt_send, rt_recv, out_sem,
 ):
@@ -138,6 +138,11 @@
         return remote(part.at[0, core, :, col(j)], z_in.at[src], pz_send.at[src], pz_recv.at[src],
                       2 * src + core, j)
 
+    def pair_row(d, _):
+        pair_w[d] = jnp.sum(
+            jnp.where(ids[...] == d, probs[...].astype(F32), 0.0), axis=0, keepdims=True)
+        return 0
+
     for n in range(2):
         loads[n].wait()
         @pl.when(lvl + 1 < levels)
@@ -147,6 +152,8 @@
         def _():
             z_copy(n, lvl, 0).start()
         core_copy(n, lvl, core).start()
+
+    lax.fori_loop(0, ep, pair_row, 0)
 
     def w_start(n, _):
         w_copy(lax.rem(e + n, ep)).start()
@@ -274,14 +281,15 @@
 
         def column(n, _):
             cs = pl.ds(pl.multiple_of(n * tile, tile), tile)
-            totals[k, :, cs] = jnp.dot(grads[k], rows[k // 2, :, cs], preferred_element_type=F32)
+            totals[k, :, cs] = jnp.dot(
+                grads[k], rows[k // 2, :, cs], preferred_element_type=F32).astype(BF16)
             return 0
 
         lax.fori_loop(0, width // tile, column, 0)
         out_copy(k).start()
 
     compute(0)
-    d_comp = nb + 2
+    d_comp = nb + 1
     last = levels - 1 + d_comp
 
     def tick(t, _):
@@ -292,18 +300,18 @@
         def back(late):
             return jnp.where(t == 1 + late, 0, jnp.where(t > d_comp + late, t - d_comp - late, -1))
 
+        for k in range(3):
+            @pl.when(t == last + k)
+            def _():
+                weight_grad(k)
         stage(drain, back(nb + 1), 0)
+        for s in range(nb, 0, -1):
+            stage(functools.partial(spread, s=s), t - s, 1)
+        stage(arrive, t, 1)
         for s in range(nb - 1, -1, -1):
             stage(functools.partial(merge_tp, s=s), back(1 + s), 0)
-        stage(arrive, t, 1)
-        for s in range(1, nb + 1):
-            stage(functools.partial(spread, s=s), t - s, 1)
         stage(compute, t - d_comp + 1, 1)
         stage(merge_core, back(0), 0)
-        for k in range(3):
-            @pl.when(t == last + k)
-            def _():
-                weight_grad(k)
         return 0
 
     lax.fori_loop(1, levels + d_comp + nb + 1, tick, 0)
@@ -340,7 +348,12 @@
     lax.fori_loop(0, levels, pz_drain, 0)
     dx_out[...] = jnp.sum(z_in[...].astype(F32), axis=0).astype(BF16)
     lax.fori_loop(1, tp, rt_wait, 0)
-    route_out[...] = jnp.sum(r_tp[...], axis=0)
+    r_in[...] = jnp.sum(r_tp[...], axis=0)
+
+    def choose(d, acc):
+        return acc + jnp.where(ids[...] == d, r_in[d], 0.0)
+
+    route_out[...] = lax.fori_loop(0, ep, choose, jnp.zeros(route_out.shape, F32))
 
     for a in range(2):
         @pl.when(lvl + 1 < levels)
@@ -384,22 +397,20 @@
     levels = ep // 2
     span = width // tp
     slots = min(levels, 8)
-    named = expert_ids.T[:, None, :] == jnp.arange(ep, dtype=jnp.int32)[None, :, None]
-    pair_w = jnp.sum(jnp.where(named, route_weight.T[:, None, :].astype(F32), 0.0), axis=0)
-    pair_w = pair_w.reshape(ep, 1, t_rows)
     any_, vmem = pl.BlockSpec(memory_space=pl.ANY), pl.BlockSpec(memory_space=pltpu.VMEM)
     dma = pltpu.SemaphoreType.DMA
-    big = jax.ShapeDtypeStruct((f_rows, width), F32)
+    big = jax.ShapeDtypeStruct((f_rows, width), BF16)
     scratch = [
         pltpu.VMEM((2, ep * t_rows, width), BF16),
         pltpu.VMEM((3, f_rows, width), BF16),
+        pltpu.VMEM((ep, 1, t_rows), F32),
         pltpu.VMEM((ep, 1, t_rows), F32),
         pltpu.VMEM((slots, 2, t_rows, width), BF16),
         pltpu.VMEM((levels, t_rows, width), BF16),
         pltpu.VMEM((levels, 2, tp - 1, t_rows // 2, span), BF16),
         pltpu.VMEM((levels, t_rows, span), BF16),
         pltpu.VMEM((3, f_rows, ep * t_rows), BF16),
-        pltpu.VMEM((3, f_rows, width), F32),
+        pltpu.VMEM((3, f_rows, width), BF16),
         pltpu.VMEM((ep, 1, t_rows), F32),
         pltpu.VMEM((ep, 1, t_rows), F32),
         pltpu.VMEM((tp, ep, 1, t_rows), F32),
@@ -412,15 +423,15 @@
         functools.partial(kernel, ep, tp),
         out_shape=(
             jax.ShapeDtypeStruct((t_rows, span), BF16),
-            jax.ShapeDtypeStruct((ep, 1, t_rows), F32), big, big, big),
-        in_specs=[any_, any_, vmem, any_, any_, any_],
+            jax.ShapeDtypeStruct(expert_ids.shape[::-1], F32), big, big, big),
+        in_specs=[any_, any_, vmem, vmem, any_, any_, any_],
         out_specs=(vmem, vmem, any_, any_, any_),
         scratch_shapes=scratch,
         compiler_params=pltpu.CompilerParams(
             collective_id=0, has_side_effects=True, vmem_limit_bytes=66_000_000),
-    )(tokens, cotangent, pair_w, gate_weight[0], up_weight[0], down_weight[0])
-    route_grad = jnp.sum(jnp.where(named, route[None, :, 0, :], 0.0), axis=1).T
-    return dx, route_grad, gate_grad[None], up_grad[None], down_grad[None]
+    )(tokens, cotangent, expert_ids.T, route_weight.T, gate_weight[0], up_weight[0], down_weight[0])
+    wide = [g.astype(F32)[None] for g in (gate_grad, up_grad, down_grad)]
+    return dx, route.T, *wide
 
 
 def solution(mesh):

time: 93.2 us -> 80.5 us (0.86)
  Pallas kernels: 80.5 us -> 72.7 us
  local copies, waits for them, and re-layouts: 8.52 us -> 1.23 us
  other arithmetic: 3.19 us -> 5.72 us
    pallas_call x1, Pallas kernels: 80.5 us -> 72.7 us  [per_device(): pl.pallas_call(functools.partial(kernel, ep, tp), out_shape=(jax.ShapeDty...]
    unnamed x10 -> x8, local copies, waits for them, and re-layouts: 8.52 us -> 1.23 us
    broadcast_in_dim x0 -> x2, other arithmetic: none -> 5.72 us  [per_device(): wide = [g.astype(F32)[None] for g in (gate_grad, up_grad, down_grad)]]
    reduce_sum x2 -> x0, other arithmetic: 2.53 us -> none  [the longest x1 1.28 us: per_device(): jnp.sum(jnp.where(named, route_weight.T[:, None, :].astype(F32), 0.0), ax...]
where the time goes in v2:
time: 80.5 us; the launch traced here: 80.3 us
  Pallas kernels  72.7 us (90%)
  other arithmetic  5.72 us (7%)
  local copies, waits for them, and re-layouts  1.23 us (2%)
    pallas_call x1, Pallas kernels, per_device(): pl.pallas_call(functools.partial(kernel, ep, tp), out_shape=(jax.ShapeDty...  72.7 us
    broadcast_in_dim x2, other arithmetic, per_device(): wide = [g.astype(F32)[None] for g in (gate_grad, up_grad, down_grad)]  5.72 us

profile of v2, /device:TPU:0, one launch (start us, length us, event | category | flops | bytes accessed | tf_op | source)
XLA Modules:
  0.0 80.3 jit_solution(11235282421655570597)
XLA Ops:
  0.6 72.7 %shard_map.110 = (bf16[128,512]{1,0:T(8,128)(2,1)}, f32[2,128]{1,0:T(2,128)}, bf16[256,2048]{1,0:T(8,128)(2,1)}, bf16[256,2048]{1,0:T(8,128)(2,1)}, bf16[256,2048]{1,0:T(8,128)(2,1)}) custom-call(bf16[128,2048]{1,0:T(8,128)(2,1)} %tokens.1, bf16[128,2048]{1,0:T(8,128)(2,1)} %cotangent.1, s32[2,128]{1,0:T(2,128)} %bitcast.18, bf16[2,128]{1,0:T(2,128)(2,1)} %bitcast.20, ...), custom_call_target="tpu_custom_call" | custom-call | tf_op jit(solution)/shard_map/pallas_call | solution.py:422
  73.3 0.0 copy-start
  73.3 4.2 %bitcast_convert_fusion = (f32[1,256,2048]{2,1,0:T(8,128)}, f32[1,256,2048]{2,1,0:T(8,128)}) fusion(bf16[256,2048]{1,0:T(8,128)(2,1)} %get-tuple-element.14, bf16[256,2048]{1,0:T(8,128)(2,1)} %get-tuple-element.13), kind=kLoop, calls=%fused_computation | loop fusion | flops 1048576 | bytes 6291456 | tf_op jit(solution)/shard_map/broadcast_in_dim | solution.py:433
  77.5 0.0 copy-start.1
  77.5 0.0 copy-start.2
  77.5 0.0 copy-done
  77.5 1.6 %bitcast_convert_fusion.2 = f32[1,256,2048]{2,1,0:T(8,128)} fusion(bf16[256,2048]{1,0:T(8,128)(2,1)S(1)} %copy-done), kind=kLoop, calls=%fused_computation.2 | loop fusion | flops 524288 | bytes 3145728 | tf_op jit(solution)/shard_map/broadcast_in_dim | solution.py:433
  79.1 0.0 copy-done.1
  79.1 0.7 copy.14
  79.7 0.0 copy-done.2
  79.7 0.6 copy.15
Async XLA Ops:
  73.3 4.2 %copy-start = (bf16[256,2048]{1,0:T(8,128)(2,1)S(1)}, bf16[256,2048]{1,0:T(8,128)(2,1)}, u32[]{:S(2)}) copy-start(bf16[256,2048]{1,0:T(8,128)(2,1)} %get-tuple-element.12) | copy-start | bytes 3145732
  77.5 1.6 %copy-start.1 = (bf16[128,512]{1,0:T(8,128)(2,1)S(1)}, bf16[128,512]{1,0:T(8,128)(2,1)}, u32[]{:S(2)}) copy-start(bf16[128,512]{1,0:T(8,128)(2,1)} %get-tuple-element.22) | copy-start | bytes 393220
  77.5 2.2 %copy-start.2 = (f32[2,128]{1,0:T(2,128)S(1)}, f32[2,128]{1,0:T(2,128)}, u32[]{:S(2)}) copy-start(f32[2,128]{1,0:T(2,128)} %get-tuple-element.11) | copy-start | bytes 3076
